TPU v7x, 32 devices: a whole 2x2x4 slice. The times are simulated.
32 devices in a mesh: grp: 2 (over y), ep: 8 (over z, x), tp: 2 (over core).
Axes of the slice: x: 2, y: 2, z: 4, core: 2. Of those that a mesh axis runs over, the one named last changes fastest.
Arguments:
- tokens: bfloat16 [4096, 2048], P(('grp', 'ep'), 'tp'), parts along dimension 0, may hold values from -6 to 6
- norm_gain: bfloat16 [2048], P('tp'), may hold values from 0.099609375 to 1.8984375
- w_gate: bfloat16 [8, 2048, 1024], P('ep', None, 'tp'), may hold values from -0.125 to 0.125
- w_up: bfloat16 [8, 2048, 1024], P('ep', None, 'tp'), may hold values from -0.125 to 0.125
- w_down: bfloat16 [8, 1024, 2048], P('ep', 'tp'), may hold values from -0.1875 to 0.1875
- expert_ids: int32 [4096, 2], P(('grp', 'ep')), parts along dimension 0, may hold values from 0 to 7, as said below
- combine: float32 [4096, 2], P(('grp', 'ep')), parts along dimension 0, may hold values from 0.1 to 1
- final_gain: bfloat16 [2048], P('tp'), may hold values from 0.099609375 to 1.8984375
Outputs:
- result: bfloat16 [4096, 2048], P(('grp', 'ep'), 'tp'), parts along dimension 0
There are 2 independent parts, one for each index of `grp`. A program takes and returns all parts, laid end to end along the dimension named above; an argument that names none is the same for every part. Nothing has to cross between parts.
Inputs may be any that keep to these rules, and one draw needn't show every extreme that they name: `expert_ids`: the experts form 4 groups of consecutive ids of equal size; the 2 experts of a row are different and lie in one group. Among the rows of one index of ep no expert is named more than 160 times, and in each such block some expert is named exactly 160 times.
All inputs are finite; a program needn't handle non-finite values.
Results may differ from a plain program's by a relative error of at most 0.0077.
Values may be sent and summed in bfloat16 or wider, within the bound.
A program may use at most 64 MiB of HBM per device.

v0:
```python
import jax
import jax.numpy as jnp
from jax import lax
from jax.sharding import PartitionSpec as P

GROUPS = 4


def body(tokens, norm_gain, w_gate, w_up, w_down, expert_ids, combine, final_gain):
    eps = 1e-06
    tok_dev, half = tokens.shape
    n_ep = lax.axis_size("ep")
    n_tp = lax.axis_size("tp")
    width = half * n_tp
    exp_dev = w_gate.shape[0]
    experts = exp_dev * n_ep
    per_group = experts // GROUPS
    capacity = tok_dev // 8 * 5 * 2 // per_group
    top = expert_ids.shape[1]
    narrow = tokens.astype(jnp.float32)
    squares = lax.psum(jnp.sum(narrow * narrow, axis=1), "tp")
    scale = lax.rsqrt(squares[:, None] / width + eps)
    normed = (narrow * scale * norm_gain.astype(jnp.float32)).astype(jnp.bfloat16)
    columns = normed.shape[1]
    flat = expert_ids.reshape(-1)
    onehot = (flat[:, None] == jnp.arange(experts, dtype=jnp.int32)[None, :]).astype(jnp.int32)
    ranking = jnp.sum(jnp.cumsum(onehot, axis=0) * onehot, axis=1) - 1
    target = flat * capacity + ranking
    sources = jnp.arange(tok_dev * top, dtype=jnp.int32) // top
    owner = jnp.full((experts * capacity,), tok_dev, jnp.int32).at[target].set(sources)
    padded = jnp.concatenate([normed, jnp.zeros((1, columns), jnp.bfloat16)], axis=0)
    outgoing = padded[owner].reshape(n_ep, exp_dev * capacity, columns)
    arrived = lax.all_to_all(outgoing, "ep", split_axis=0, concat_axis=0, tiled=True)
    rows = (
        arrived.reshape(n_ep, exp_dev, capacity, columns)
        .transpose(1, 0, 2, 3)
        .reshape(exp_dev, n_ep * capacity, columns)
    )
    piece = lax.all_gather(rows, "tp", axis=2, tiled=True)
    gate = jnp.einsum("erd,edf->erf", piece, w_gate, preferred_element_type=jnp.float32)
    upper = jnp.einsum("erd,edf->erf", piece, w_up, preferred_element_type=jnp.float32)
    hidden = (jax.nn.silu(gate) * upper).astype(jnp.bfloat16)
    partial_out = jnp.einsum(
        "erf,efd->erd", hidden, w_down, preferred_element_type=jnp.float32
    ).astype(jnp.bfloat16)
    shares = (
        lax.psum_scatter(partial_out, "tp", scatter_dimension=2, tiled=True)
        .astype(jnp.float32)
        .astype(jnp.bfloat16)
    )
    homeward = (
        shares.reshape(exp_dev, n_ep, capacity, half)
        .transpose(1, 0, 2, 3)
        .reshape(n_ep, exp_dev * capacity, half)
    )
    returned = lax.all_to_all(homeward, "ep", split_axis=0, concat_axis=0, tiled=True).reshape(
        experts * capacity, half
    )
    picked = returned[target].astype(jnp.float32).reshape(tok_dev, top, half)
    mixed = jnp.sum(picked * combine[:, :, None], axis=1)
    totals = lax.psum(jnp.sum(mixed * mixed, axis=1), "tp")
    norm = lax.rsqrt(totals[:, None] / width + eps)
    return (mixed * norm * final_gain.astype(jnp.float32)).astype(jnp.bfloat16)


def solution(mesh):
    placed = (
        P(("grp", "ep"), "tp"),
        P("tp"),
        P("ep", None, "tp"),
        P("ep", None, "tp"),
        P("ep", "tp", None),
        P(("grp", "ep"), None),
        P(("grp", "ep"), None),
        P("tp"),
    )
    return jax.shard_map(
        body, mesh=mesh, in_specs=placed, out_specs=P(("grp", "ep"), "tp"), check_vma=False
    )
```

profile of v0, /device:TPU:0, one launch (start us, length us, event | category | flops | bytes accessed | tf_op | source)
XLA Modules:
  0.0 225.1 jit_solution(16053872975609984581)
XLA Ops:
  6.5 1.0 copy.11
  7.5 0.1 eq.29
  7.7 0.1 eq.25
  7.8 0.7 broadcast_multiply_fusion
  8.5 1.1 reduce-window.6
  9.6 0.2 slice_reduce_fusion
  9.9 0.1 fusion.21
  10.0 0.1 copy.10
  10.1 0.1 mul.81
  10.3 2.5 %scatter_custom_fusion = s32[1280]{0:T(1024)S(1)} fusion(s32[512]{0:T(512)S(1)} %bitcast.39, s32[512]{0:T(512)S(1)} %add_select_fusion, s32[]{:T(128)} %constant.38.clone.1), kind=kCustom, calls=%fused_computation.35 | custom fusion | bytes 5124 | tf_op jit(solution)/shard_map/scatter | solution.py:30
  12.8 0.7 convert_element_type.40
  13.5 1.2 fusion.18
  14.7 2.6 %psum.14 = f32[256]{0:T(256)S(1)} all-reduce(f32[256]{0:T(256)S(1)} %fusion.18), channel_id=1, replica_groups=mesh['grp'=2,'ep'=8,'tp'=2] {'tp'}, use_global_device_ids=true, to_apply=%region_1.0 | all-reduce | flops 256 | bytes 2048 | tf_op jit(solution)/shard_map/psum | solution.py:21
  17.3 1.2 fusion.20
  18.6 5.1 %gather_fusion = bf16[1280,1024]{1,0:T(8,128)(2,1)} fusion(bf16[257,1024]{1,0:T(8,128)(2,1)S(1)} %concatenate.3, s32[2048]{0:T(1024)S(1)} %pad_clamp_fusion), kind=kCustom, calls=%fused_computation | custom fusion | bytes 5248000 | tf_op jit(solution)/shard_map/gather | solution.py:32
  23.7 67.0 %all_to_all.10 = bf16[8,160,1024]{2,1,0:T(8,128)(2,1)} all-to-all(bf16[8,160,1024]{2,1,0:T(8,128)(2,1)} %bitcast.37), channel_id=1, replica_groups=mesh['grp'=2,'ep'=8,'tp'=2] {'ep'}, dimensions={0} | all-to-all | bytes 5242880 | tf_op jit(solution)/shard_map/all_to_all | solution.py:33
  90.7 0.0 all-gather.2.cloned.1.call-update
  90.7 0.0 reduce-scatter.2.cloned.1.call-start
  90.8 14.4 %all-gather.2.cloned.1.call-done = bf16[1,1280,2048]{2,1,0:T(8,128)(2,1)} async-done(((bf16[1,1280,1024]{2,1,0:T(8,128)(2,1)}), bf16[1,1280,2048]{2,1,0:T(8,128)(2,1)}) %all-gather.2.cloned.1.call-update) | async-done | bytes 5242896 | tf_op jit(solution)/shard_map/all_gather | solution.py:39
  105.2 7.6 %fusion.3 = f32[1280,512]{1,0:T(8,128)} fusion(bf16[1,1280,2048]{2,1,0:T(8,128)(2,1)} %all-gather.2.cloned.1.call-done, bf16[1,2048,512]{2,1,0:T(8,128)(2,1)} %param.10), kind=kOutput, calls=%fused_computation.7 | convolution fusion | flops 2684354560 | bytes 9961472 | tf_op jit(solution)/shard_map/erd,edf->erf/dot_general | solution.py:40
  112.7 10.3 %fusion = bf16[1,1280,2048]{2,1,0:T(8,128)(2,1)} fusion(bf16[1,512,2048]{2,1,0:T(8,128)(2,1)S(1)} %copy-done, bf16[1,1280,2048]{2,1,0:T(8,128)(2,1)} %all-gather.2.cloned.1.call-done, f32[1280,512]{1,0:T(8,128)} %fusion.3, bf16[1,2048,512]{2,1,0:T(8,128)(2,1)} %param.11), kind=kOutput, calls=%fused_computation.4 | convolution fusion | flops 5375262720 | bytes 17301504 | tf_op jit(solution)/shard_map/erf,efd->erd/dot_general | solution.py:43
  123.1 0.0 reduce-scatter.2.cloned.1.call-update
  123.1 14.2 %reduce-scatter.2.cloned.1.call-done = bf16[1,1280,1024]{2,1,0:T(8,128)(2,1)} async-done(((bf16[1,1280,2048]{2,1,0:T(8,128)(2,1)}), bf16[1,1280,1024]{2,1,0:T(8,128)(2,1)}) %reduce-scatter.2.cloned.1.call-update) | async-done | bytes 2621456 | tf_op jit(solution)/shard_map/reduce_scatter | solution.py:47
  137.3 6.0 %all-to-all-start.1 = ((bf16[8,160,1024]{2,1,0:T(8,128)(2,1)}), bf16[8,160,1024]{2,1,0:T(8,128)(2,1)}, u32[]{:S(2)}, u32[]{:S(2)}) async-start(bf16[8,160,1024]{2,1,0:T(8,128)(2,1)} %bitcast.38), calls=%async_computation.2 | async-start | bytes 5242880 | tf_op jit(solution)/shard_map/all_to_all | solution.py:56
  143.3 0.1 copy.13
  143.5 59.7 %all-to-all-done.1 = bf16[8,160,1024]{2,1,0:T(8,128)(2,1)} async-done(((bf16[8,160,1024]{2,1,0:T(8,128)(2,1)}), bf16[8,160,1024]{2,1,0:T(8,128)(2,1)}, u32[]{:S(2)}, u32[]{:S(2)}) %all-to-all-start.1) | async-done | bytes 2621472 | tf_op jit(solution)/shard_map/all_to_all | solution.py:56
  203.2 4.8 %gather_fusion.1 = bf16[512,1024]{1,0:T(8,128)(2,1)S(1)} fusion(bf16[1280,1024]{1,0:T(8,128)(2,1)} %bitcast.12, s32[1024]{0:T(1024)S(1)} %pad_clamp_fusion.1), kind=kCustom, calls=%fused_computation.1 | custom fusion | bytes 2099200 | tf_op jit(solution)/shard_map/gather | solution.py:59
  208.0 2.4 %reshape.105 = f32[256,2,1024]{2,1,0:T(2,128)} reshape(bf16[512,1024]{1,0:T(8,128)(2,1)S(1)} %gather_fusion.1) | data formatting | bytes 3145728 | tf_op jit(solution)/shard_map/convert_element_type | solution.py:59
  210.4 4.3 %multiply_reduce_fusion = f32[256,1024]{1,0:T(8,128)S(1)} fusion(f32[256,2,1024]{2,1,0:T(2,128)} %reshape.105, f32[256,2]{1,0:T(8,128)S(1)} %copy.13), kind=kLoop, calls=%fused_computation.14 | loop fusion | flops 786432 | bytes 3147776 | tf_op jit(solution)/shard_map/reduce_sum | solution.py:60
  214.7 0.1 multiply_reduce_fusion.1
  214.8 2.5 %psum.15 = f32[256]{0:T(256)S(1)} all-reduce(f32[256]{0:T(256)S(1)} %multiply_reduce_fusion.1), channel_id=1, replica_groups=mesh['grp'=2,'ep'=8,'tp'=2] {'tp'}, use_global_device_ids=true, to_apply=%region_9.10 | all-reduce | flops 256 | bytes 2048 | tf_op jit(solution)/shard_map/psum | solution.py:61
  217.3 1.0 multiply_convert_fusion
  (20 shorter events, 0.1 us)
Async XLA Ops:
  6.5 106.2 %copy-start = (bf16[1,512,2048]{2,1,0:T(8,128)(2,1)S(1)}, bf16[1,512,2048]{2,1,0:T(8,128)(2,1)}, u32[]{:S(2)}) copy-start(bf16[1,512,2048]{2,1,0:T(8,128)(2,1)} %param.12) | copy-start | bytes 6291460
  6.5 98.6 %all-gather.2.cloned.1.call-start = ((), (), s32[]{:S(2)}) async-start(), calls=%async_computation.3 | async-start | bytes 7864320 | tf_op jit(solution)/shard_map/all_gather | solution.py:39
  90.7 46.6 %reduce-scatter.2.cloned.1.call-start = ((), (), s32[]{:S(2)}) async-start(), calls=%async_computation.4 | async-start | bytes 7864320 | tf_op jit(solution)/shard_map/reduce_scatter | solution.py:47
  137.3 6.0 %copy-start.1 = (f32[256,2]{0,1:T(2,128)S(1)}, f32[256,2]{0,1:T(2,128)}, u32[]{:S(2)}) copy-start(f32[256,2]{0,1:T(2,128)} %param.14) | copy-start | bytes 6148
  137.3 6.2 %copy-start.2 = (bf16[1024]{0:T(1024)(128)(2,1)S(1)}, bf16[1024]{0:T(1024)(128)(2,1)}, u32[]{:S(2)}) copy-start(bf16[1024]{0:T(1024)(128)(2,1)} %param.15) | copy-start | bytes 6148
  137.3 65.9 %all-to-all-start.1 = ((bf16[8,160,1024]{2,1,0:T(8,128)(2,1)}), bf16[8,160,1024]{2,1,0:T(8,128)(2,1)}, u32[]{:S(2)}, u32[]{:S(2)}) async-start(bf16[8,160,1024]{2,1,0:T(8,128)(2,1)} %bitcast.38), calls=%async_computation.2 | async-start | bytes 5242880 | tf_op jit(solution)/shard_map/all_to_all | solution.py:56
Sparse Core Ops, SparseCore 0:
  90.8 14.2 all-gather.1
  123.2 14.0 reduce-scatter.1
where the time goes:
time: 226 us; the launch traced here: 225 us
  waiting for transfers between devices  88.3 us (39%)
  blocking collectives  72.1 us (32%)
  matrix products  17.9 us (8%)
  local copies, waits for them, and re-layouts  16.6 us (7%)
  between operations  13.5 us (6%)
  other arithmetic  10.6 us (5%)
  starting transfers between devices  6.05 us (3%)
    all_to_all x1, blocking collectives, body(): lax.all_to_all(outgoing, 'ep', split_axis=0, concat_axis=0, tiled=True)  67 us
    all_to_all x1, waiting for transfers between devices, body(): lax.all_to_all(homeward, 'ep', split_axis=0, concat_axis=0, tiled=True)  59.7 us
    all_gather x1, waiting for transfers between devices, body(): piece = lax.all_gather(rows, 'tp', axis=2, tiled=True)  14.4 us
    reduce_scatter x1, waiting for transfers between devices, body(): lax.psum_scatter(partial_out, 'tp', scatter_dimension=2, tiled=True)  14.2 us
    dot_general x1, matrix products, body(): jnp.einsum('erf,efd->erd', hidden, w_down, preferred_element_type=jnp.flo...  10.3 us
    dot_general x1, matrix products, body(): jnp.einsum('erd,edf->erf', piece, w_gate, preferred_element_type=jnp.floa...  7.55 us
    all_to_all x1, starting transfers between devices, body(): lax.all_to_all(homeward, 'ep', split_axis=0, concat_axis=0, tiled=True)  6.01 us
    gather x1, local copies, waits for them, and re-layouts, body(): outgoing = padded[owner].reshape(n_ep, exp_dev * capacity, columns)  5.08 us
  transfers between devices with their start and end apart: 3, of which 3 were waited for; matrix products, arithmetic and copies ran while one was open for 0% of the time, Pallas kernels for 0%

commit v1 on v0

--- a/solution.py
+++ b/solution.py
@@ -36,7 +36,7 @@
         .transpose(1, 0, 2, 3)
         .reshape(exp_dev, n_ep * capacity, columns)
     )
-    piece = lax.all_gather(rows, "tp", axis=2, tiled=True)
+    piece = jnp.concatenate(lax.all_gather(rows, "tp"), axis=2)
     gate = jnp.einsum("erd,edf->erf", piece, w_gate, preferred_element_type=jnp.float32)
     upper = jnp.einsum("erd,edf->erf", piece, w_up, preferred_element_type=jnp.float32)
     hidden = (jax.nn.silu(gate) * upper).astype(jnp.bfloat16)

time: 226 us -> 234 us (1.035)
  local copies, waits for them, and re-layouts: 16.6 us -> 24.6 us
    all_gather x0 -> x1, local copies, waits for them, and re-layouts: none -> 7.91 us  [body(): piece = jnp.concatenate(lax.all_gather(rows, 'tp'), axis=2)]
where the time goes in v1:
time: 234 us; the launch traced here: 233 us
  waiting for transfers between devices  88.4 us (38%)
  blocking collectives  72.1 us (31%)
  local copies, waits for them, and re-layouts  24.6 us (11%)
  matrix products  17.9 us (8%)
  between operations  13.5 us (6%)
  other arithmetic  10.5 us (4%)
  starting transfers between devices  6.04 us (3%)
    all_to_all x1, blocking collectives, body(): lax.all_to_all(outgoing, 'ep', split_axis=0, concat_axis=0, tiled=True)  67 us
    all_to_all x1, waiting for transfers between devices, body(): lax.all_to_all(homeward, 'ep', split_axis=0, concat_axis=0, tiled=True)  59.7 us
    all_gather x1, waiting for transfers between devices, body(): piece = jnp.concatenate(lax.all_gather(rows, 'tp'), axis=2)  14.4 us
    reduce_scatter x1, waiting for transfers between devices, body(): lax.psum_scatter(partial_out, 'tp', scatter_dimension=2, tiled=True)  14.2 us
    dot_general x1, matrix products, body(): jnp.einsum('erf,efd->erd', hidden, w_down, preferred_element_type=jnp.flo...  10.3 us
    all_gather x1, local copies, waits for them, and re-layouts, body(): piece = jnp.concatenate(lax.all_gather(rows, 'tp'), axis=2)  7.91 us
    dot_general x1, matrix products, body(): jnp.einsum('erd,edf->erf', piece, w_gate, preferred_element_type=jnp.floa...  7.58 us
    all_to_all x1, starting transfers between devices, body(): lax.all_to_all(homeward, 'ep', split_axis=0, concat_axis=0, tiled=True)  6 us
  transfers between devices with their start and end apart: 3, of which 3 were waited for; matrix products, arithmetic and copies ran while one was open for 0% of the time, Pallas kernels for 0%

profile of v1, /device:TPU:0, one launch (start us, length us, event | category | flops | bytes accessed | tf_op | source)
XLA Modules:
  0.0 233.1 jit_solution(17328793003309246335)
XLA Ops:
  6.5 1.0 copy.21
  7.5 0.1 eq.29
  7.7 0.1 eq.25
  7.8 0.7 broadcast_multiply_fusion
  8.5 1.1 reduce-window.6
  9.6 0.2 slice_reduce_fusion
  9.9 0.1 fusion.11
  10.0 0.1 copy.20
  10.1 0.1 mul.81
  10.3 2.5 %scatter_custom_fusion = s32[1280]{0:T(1024)S(1)} fusion(s32[512]{0:T(512)S(1)} %bitcast.35, s32[512]{0:T(512)S(1)} %add_select_fusion, s32[]{:T(128)} %constant.38.clone.1), kind=kCustom, calls=%fused_computation.32 | custom fusion | bytes 5124 | tf_op jit(solution)/shard_map/scatter | solution.py:30
  12.8 0.7 convert_element_type.40
  13.5 1.2 fusion.6
  14.7 2.6 %psum.14 = f32[256]{0:T(256)S(1)} all-reduce(f32[256]{0:T(256)S(1)} %fusion.6), channel_id=1, replica_groups=mesh['grp'=2,'ep'=8,'tp'=2] {'tp'}, use_global_device_ids=true, to_apply=%region_1.0 | all-reduce | flops 256 | bytes 2048 | tf_op jit(solution)/shard_map/psum | solution.py:21
  17.3 1.2 fusion.8
  18.6 5.1 %gather_fusion = bf16[1280,1024]{1,0:T(8,128)(2,1)} fusion(bf16[257,1024]{1,0:T(8,128)(2,1)S(1)} %concatenate.3, s32[2048]{0:T(1024)S(1)} %pad_clamp_fusion), kind=kCustom, calls=%fused_computation | custom fusion | bytes 5248000 | tf_op jit(solution)/shard_map/gather | solution.py:32
  23.7 67.0 %all_to_all.10 = bf16[8,160,1024]{2,1,0:T(8,128)(2,1)} all-to-all(bf16[8,160,1024]{2,1,0:T(8,128)(2,1)} %bitcast.31), channel_id=1, replica_groups=mesh['grp'=2,'ep'=8,'tp'=2] {'ep'}, dimensions={0} | all-to-all | bytes 5242880 | tf_op jit(solution)/shard_map/all_to_all | solution.py:33
  90.7 0.0 all-gather.2.cloned.1.call-update
  90.7 0.0 reduce-scatter.2.cloned.1.call-start
  90.8 14.4 %all-gather.2.cloned.1.call-done = bf16[2,1,1280,1024]{3,2,1,0:T(8,128)(2,1)} async-done(((bf16[1,1,1280,1024]{3,2,1,0:T(8,128)(2,1)}), bf16[2,1,1280,1024]{3,2,1,0:T(8,128)(2,1)}) %all-gather.2.cloned.1.call-update) | async-done | bytes 5242896 | tf_op jit(solution)/shard_map/all_gather | solution.py:39
  105.2 7.9 %copy.23 = bf16[2,1,1280,1024]{2,3,0,1:T(8,128)(2,1)} copy(bf16[2,1,1280,1024]{3,2,1,0:T(8,128)(2,1)} %all-gather.2.cloned.1.call-done) | data formatting | bytes 10485760 | tf_op jit(solution)/shard_map/all_gather | solution.py:39
  113.1 7.6 %fusion.4 = f32[1280,512]{1,0:T(8,128)} fusion(bf16[1280,2048]{0,1:T(8,128)(2,1)} %bitcast.32, bf16[1,2048,512]{2,1,0:T(8,128)(2,1)} %param.10), kind=kOutput, calls=%fused_computation.9 | convolution fusion | flops 2684354560 | bytes 9961472 | tf_op jit(solution)/shard_map/erd,edf->erf/dot_general | solution.py:40
  120.7 10.3 %fusion = bf16[1,1280,2048]{2,1,0:T(8,128)(2,1)} fusion(bf16[1,512,2048]{2,1,0:T(8,128)(2,1)S(1)} %copy-done, bf16[1280,2048]{0,1:T(8,128)(2,1)} %bitcast.33, f32[1280,512]{1,0:T(8,128)} %fusion.4, bf16[1,2048,512]{2,1,0:T(8,128)(2,1)} %param.11), kind=kOutput, calls=%fused_computation.4 | convolution fusion | flops 5375262720 | bytes 17301504 | tf_op jit(solution)/shard_map/erf,efd->erd/dot_general | solution.py:43
  131.1 14.2 %reduce-scatter.2.cloned.1.call-done = bf16[1,1280,1024]{2,1,0:T(8,128)(2,1)} async-done(((bf16[1,1280,2048]{2,1,0:T(8,128)(2,1)}), bf16[1,1280,1024]{2,1,0:T(8,128)(2,1)}) %reduce-scatter.2.cloned.1.call-update) | async-done | bytes 2621456 | tf_op jit(solution)/shard_map/reduce_scatter | solution.py:47
  145.3 6.0 %all-to-all-start.1 = ((bf16[8,160,1024]{2,1,0:T(8,128)(2,1)}), bf16[8,160,1024]{2,1,0:T(8,128)(2,1)}, u32[]{:S(2)}, u32[]{:S(2)}) async-start(bf16[8,160,1024]{2,1,0:T(8,128)(2,1)} %bitcast.34), calls=%async_computation.2 | async-start | bytes 5242880 | tf_op jit(solution)/shard_map/all_to_all | solution.py:56
  151.3 0.1 copy.24
  151.4 59.7 %all-to-all-done.1 = bf16[8,160,1024]{2,1,0:T(8,128)(2,1)} async-done(((bf16[8,160,1024]{2,1,0:T(8,128)(2,1)}), bf16[8,160,1024]{2,1,0:T(8,128)(2,1)}, u32[]{:S(2)}, u32[]{:S(2)}) %all-to-all-start.1) | async-done | bytes 2621472 | tf_op jit(solution)/shard_map/all_to_all | solution.py:56
  211.2 4.8 %gather_fusion.1 = bf16[512,1024]{1,0:T(8,128)(2,1)S(1)} fusion(bf16[1280,1024]{1,0:T(8,128)(2,1)} %bitcast.14, s32[1024]{0:T(1024)S(1)} %pad_clamp_fusion.1), kind=kCustom, calls=%fused_computation.1 | custom fusion | bytes 2099200 | tf_op jit(solution)/shard_map/gather | solution.py:59
  216.0 2.4 %reshape.112 = f32[256,2,1024]{2,1,0:T(2,128)} reshape(bf16[512,1024]{1,0:T(8,128)(2,1)S(1)} %gather_fusion.1) | data formatting | bytes 3145728 | tf_op jit(solution)/shard_map/convert_element_type | solution.py:59
  218.4 4.3 %multiply_reduce_fusion = f32[256,1024]{1,0:T(8,128)S(1)} fusion(f32[256,2,1024]{2,1,0:T(2,128)} %reshape.112, f32[256,2]{1,0:T(8,128)S(1)} %copy.24), kind=kLoop, calls=%fused_computation.11 | loop fusion | flops 786432 | bytes 3147776 | tf_op jit(solution)/shard_map/reduce_sum | solution.py:60
  222.7 0.1 multiply_reduce_fusion.1
  222.8 2.5 %psum.15 = f32[256]{0:T(256)S(1)} all-reduce(f32[256]{0:T(256)S(1)} %multiply_reduce_fusion.1), channel_id=1, replica_groups=mesh['grp'=2,'ep'=8,'tp'=2] {'tp'}, use_global_device_ids=true, to_apply=%region_9.10 | all-reduce | flops 256 | bytes 2048 | tf_op jit(solution)/shard_map/psum | solution.py:61
  225.3 1.0 multiply_convert_fusion
  (21 shorter events, 0.2 us)
Async XLA Ops:
  6.5 114.2 %copy-start = (bf16[1,512,2048]{2,1,0:T(8,128)(2,1)S(1)}, bf16[1,512,2048]{2,1,0:T(8,128)(2,1)}, u32[]{:S(2)}) copy-start(bf16[1,512,2048]{2,1,0:T(8,128)(2,1)} %param.12) | copy-start | bytes 6291460
  6.5 98.7 %all-gather.2.cloned.1.call-start = ((), (), s32[]{:S(2)}) async-start(), calls=%async_computation.3 | async-start | bytes 7864320 | tf_op jit(solution)/shard_map/all_gather | solution.py:39
  90.7 54.5 %reduce-scatter.2.cloned.1.call-start = ((), (), s32[]{:S(2)}) async-start(), calls=%async_computation.4 | async-start | bytes 7864320 | tf_op jit(solution)/shard_map/reduce_scatter | solution.py:47
  145.3 6.0 %copy-start.1 = (f32[256,2]{0,1:T(2,128)S(1)}, f32[256,2]{0,1:T(2,128)}, u32[]{:S(2)}) copy-start(f32[256,2]{0,1:T(2,128)} %param.14) | copy-start | bytes 6148
  145.3 6.2 %copy-start.2 = (bf16[1024]{0:T(1024)(128)(2,1)S(1)}, bf16[1024]{0:T(1024)(128)(2,1)}, u32[]{:S(2)}) copy-start(bf16[1024]{0:T(1024)(128)(2,1)} %param.15) | copy-start | bytes 6148
  145.3 65.9 %all-to-all-start.1 = ((bf16[8,160,1024]{2,1,0:T(8,128)(2,1)}), bf16[8,160,1024]{2,1,0:T(8,128)(2,1)}, u32[]{:S(2)}, u32[]{:S(2)}) async-start(bf16[8,160,1024]{2,1,0:T(8,128)(2,1)} %bitcast.34), calls=%async_computation.2 | async-start | bytes 5242880 | tf_op jit(solution)/shard_map/all_to_all | solution.py:56
Sparse Core Ops, SparseCore 0:
  90.9 14.2 all-gather.1
  131.2 14.0 reduce-scatter.1
